TPU v7x, 32 devices: a whole 2x2x4 slice. The times are simulated.
32 devices in a mesh: kv: 8 (over z, y), tp: 4 (over x, core).
Axes of the slice: x: 2, y: 2, z: 4, core: 2. Of those that a mesh axis runs over, the one named last changes fastest.
Arguments:
- tokens: bfloat16 [32, 4096], P(None, ('kv', 'tp')), may hold values from -36 to 36
- first_gain: float32 [4096], P('kv'), may hold values from 0.1 to 1.9
- first_gate: bfloat16 [4096, 11264], P('kv', 'tp'), may hold values from -0.09375 to 0.09375
- first_up: bfloat16 [4096, 11264], P('kv', 'tp'), may hold values from -0.09375 to 0.09375
- first_down: bfloat16 [11264, 4096], P('tp', 'kv'), may hold values from -0.0546875 to 0.0546875
- mix_gain: float32 [4096], P('kv'), may hold values from 0.1 to 1.9
- w_query: bfloat16 [4096, 2048], P('kv', 'tp'), may hold values from -0.09375 to 0.09375
- key_cache: bfloat16 [32, 8192, 1024], P(None, 'kv', 'tp'), may hold values from -100 to 100
- value_cache: bfloat16 [32, 8192, 1024], P(None, 'kv', 'tp'), may hold values from -6 to 6
- map_weight: float32 [32], P('tp'), may hold values from 0.3 to 0.8
- head_gain: float32 [64], replicated, may hold values from 0.1 to 1.9
- w_out: bfloat16 [2048, 4096], P('tp', 'kv'), may hold values from -0.125 to 0.125
- second_gain: float32 [4096], P('kv'), may hold values from 0.1 to 1.9
- second_gate: bfloat16 [4096, 11264], P('kv', 'tp'), may hold values from -0.09375 to 0.09375
- second_up: bfloat16 [4096, 11264], P('kv', 'tp'), may hold values from -0.09375 to 0.09375
- second_down: bfloat16 [11264, 4096], P('tp', 'kv'), may hold values from -0.0546875 to 0.0546875
Outputs:
- mixed: bfloat16 [32, 4096], P(None, ('kv', 'tp'))
All inputs are finite; a program needn't handle non-finite values.
Results may differ from a plain program's by a relative error of at most 0.0158.
Values may be sent and summed in bfloat16 or wider, within the bound.
A program may use at most 128 MiB of HBM per device.

v0:
```python
import math
import jax
import jax.numpy as jnp
from jax import lax
from jax.sharding import PartitionSpec as P

D = 4096
HEAD = 64
EPS = 1e-06
HEAD_SCALE = 0.8


def merged(value, axis, join):
    pieces = jax.tree.map(lambda part: lax.all_gather(part, axis), value)
    head = jax.tree.map(lambda part: part[0], pieces)
    tail = jax.tree.map(lambda part: part[1:], pieces)
    subtotal, _ = lax.scan(lambda subtotal, piece: (join(subtotal, piece), None), head, tail)
    return subtotal


def norm_total(squares):
    return lax.psum(squares, "kv")


def channel_mixer(residual, gain, w_gate, w_up, w_down):
    squares = jnp.sum(residual * residual, axis=1, keepdims=True)
    scaled = (residual * gain).astype(jnp.bfloat16)
    part_gate = jnp.dot(scaled, w_gate, preferred_element_type=jnp.float32)
    part_up = jnp.dot(scaled, w_up, preferred_element_type=jnp.float32)
    row_total = norm_total(squares)
    gate_sum, up_sum = lax.psum((part_gate, part_up), "kv")
    factor = lax.rsqrt(row_total / D + EPS)
    active = (jax.nn.silu(gate_sum * factor) * (up_sum * factor)).astype(jnp.bfloat16)
    partial_value = jnp.dot(active, w_down, preferred_element_type=jnp.float32)
    return lax.psum(partial_value, "tp")


def merge_pair(first, second):
    row_peak = jnp.maximum(first[0], second[0])
    scale_first = jnp.exp(first[0] - row_peak)
    scale_second = jnp.exp(second[0] - row_peak)
    return (
        row_peak,
        first[1] * scale_first + second[1] * scale_second,
        first[2] * scale_first[..., None] + second[2] * scale_second[..., None],
    )


def combine_maps(earlier, later):
    return merge_pair(earlier[:3], later[:3]) + merge_pair(earlier[3:], later[3:])


def attention_mix(
    residual, mix_gain, w_query, key_cache, value_cache, map_weight, head_gain, w_out
):
    squares = jnp.sum(residual * residual, axis=1, keepdims=True)
    scaled = (residual * mix_gain).astype(jnp.bfloat16)
    part_query = jnp.dot(scaled, w_query, preferred_element_type=jnp.float32)
    row_total = norm_total(squares)
    queries = lax.psum(part_query, "kv")
    queries = (queries * lax.rsqrt(row_total / D + EPS)).astype(jnp.bfloat16)
    batch_rows = queries.shape[0]
    kv_local = key_cache.shape[2] // HEAD
    group = queries.shape[1] // (kv_local * HEAD)
    queries = queries.reshape(batch_rows, kv_local, group, HEAD)
    cached = key_cache.reshape(batch_rows, -1, kv_local, HEAD)
    stored = value_cache.reshape(batch_rows, -1, kv_local, HEAD)

    def partial_map(first_col, last_col):
        scores = jnp.einsum(
            "bkgd,bpkd->bkgp",
            queries[..., first_col:last_col],
            cached[..., first_col:last_col],
            preferred_element_type=jnp.float32,
        ) / math.sqrt(last_col - first_col)
        row_peak = jnp.max(scores, axis=3)
        exp_terms = jnp.exp(scores - row_peak[..., None])
        weights_sum = jnp.sum(exp_terms, axis=3)
        summed = jnp.einsum(
            "bkgp,bpkd->bkgd",
            exp_terms.astype(jnp.bfloat16),
            stored,
            preferred_element_type=jnp.float32,
        )
        return (row_peak, weights_sum, summed)

    half_dim = HEAD // 2
    peak_one, sum_one, out_one = partial_map(0, half_dim)
    peak_two, sum_two, out_two = partial_map(half_dim, HEAD)
    peak_one, sum_one, out_one, peak_two, sum_two, out_two = merged(
        (peak_one, sum_one, out_one, peak_two, sum_two, out_two), "kv", combine_maps
    )
    weight = map_weight.reshape(kv_local, group)
    combined = out_one / sum_one[..., None] - weight[..., None] * out_two / sum_two[..., None]
    normed = (
        combined
        * lax.rsqrt(jnp.mean(combined * combined, axis=3, keepdims=True) + EPS)
        * head_gain
        * HEAD_SCALE
    )
    normed = normed.astype(jnp.bfloat16).reshape(batch_rows, kv_local * group * HEAD)
    partial_value = jnp.dot(normed, w_out, preferred_element_type=jnp.float32)
    return lax.psum(partial_value, "tp")


def on_device(
    tokens,
    first_gain,
    first_gate,
    first_up,
    first_down,
    mix_gain,
    w_query,
    key_cache,
    value_cache,
    map_weight,
    head_gain,
    w_out,
    second_gain,
    second_gate,
    second_up,
    second_down,
):
    residual = lax.all_gather(tokens, "tp", axis=1, tiled=True).astype(jnp.float32)
    residual = residual + 0.5 * channel_mixer(
        residual, first_gain, first_gate, first_up, first_down
    )
    residual = residual + attention_mix(
        residual, mix_gain, w_query, key_cache, value_cache, map_weight, head_gain, w_out
    )
    residual = residual + 0.5 * channel_mixer(
        residual, second_gain, second_gate, second_up, second_down
    )
    width = residual.shape[1] // lax.axis_size("tp")
    return lax.dynamic_slice_in_dim(residual, lax.axis_index("tp") * width, width, 1).astype(
        jnp.bfloat16
    )


def solution(mesh):
    placed = (
        P(None, ("kv", "tp")),
        P("kv"),
        P("kv", "tp"),
        P("kv", "tp"),
        P("tp", "kv"),
        P("kv"),
        P("kv", "tp"),
        P(None, "kv", "tp"),
        P(None, "kv", "tp"),
        P("tp"),
        P(),
        P("tp", "kv"),
        P("kv"),
        P("kv", "tp"),
        P("kv", "tp"),
        P("tp", "kv"),
    )
    return jax.shard_map(
        on_device, mesh=mesh, in_specs=placed, out_specs=P(None, ("kv", "tp")), check_vma=False
    )
```

profile of v0, /device:TPU:0, one launch (start us, length us, event | category | flops | bytes accessed | tf_op | source)
XLA Modules:
  0.0 626.8 jit_solution(4104942960489870407)
XLA Ops:
  6.5 6.5 %all_gather.39 = bf16[32,512]{1,0:T(8,128)(2,1)S(1)} all-gather(bf16[32,128]{1,0:T(8,128)(2,1)} %param.18), channel_id=1, replica_groups=mesh['kv'=8,'tp'=4] {'tp'}, dimensions={1}, use_global_device_ids=true | all-gather | bytes 40960 | tf_op jit(solution)/shard_map/all_gather | solution.py:124
  16.6 22.7 %psum.78 = f32[32,1]{0,1:T(1,128)S(1)} all-reduce(f32[32,1]{0,1:T(1,128)S(1)} %bitcast.79), channel_id=1, replica_groups=mesh['kv'=8,'tp'=4] {'kv'}, use_global_device_ids=true, to_apply=%region_2.0 | all-reduce | flops 32 | bytes 256 | tf_op jit(solution)/shard_map/psum | solution.py:22
  39.3 53.8 %all-reduce.19.cloned.1.call-done = (f32[32,2816]{1,0:T(8,128)}, f32[32,2816]{1,0:T(8,128)}) async-done(((f32[32,2816]{1,0:T(8,128)}, f32[32,2816]{1,0:T(8,128)}), (f32[32,2816]{1,0:T(8,128)}, f32[32,2816]{1,0:T(8,128)})) %all-reduce.19.cloned.1.call-update) | async-done | bytes 720912 | tf_op jit(solution)/shard_map/psum | solution.py:31
  95.6 22.5 %copy.107 = bf16[32,1024,256]{1,2,0:T(8,128)(2,1)} copy(bf16[32,1024,256]{2,1,0:T(8,128)(2,1)} %param.25) | data formatting | bytes 33554432 | tf_op args[7]
  118.2 22.6 %copy.110 = bf16[32,1024,256]{1,2,0:T(8,128)(2,1)} copy(bf16[32,1024,256]{2,1,0:T(8,128)(2,1)} %param.26) | data formatting | bytes 33554432 | tf_op args[8]
  141.7 19.6 %psum.82 = f32[32,1]{0,1:T(1,128)S(1)} all-reduce(f32[32,1]{0,1:T(1,128)S(1)} %bitcast.80), channel_id=1, replica_groups=mesh['kv'=8,'tp'=4] {'kv'}, use_global_device_ids=true, to_apply=%region_7.8 | all-reduce | flops 32 | bytes 256 | tf_op jit(solution)/shard_map/psum | solution.py:22
  163.1 66.6 %all-reduce.11.cloned.1.call-done = f32[32,512]{1,0:T(8,128)} async-done(((f32[32,512]{1,0:T(8,128)}), f32[32,512]{1,0:T(8,128)}) %all-reduce.11.cloned.1.call-update) | async-done | bytes 65552 | tf_op jit(solution)/shard_map/psum | solution.py:60
  230.7 4.9 fusion.55
  235.6 4.9 fusion.54
  242.0 30.9 %all-gather.1 = f32[256,4,2]{1,2,0:T(2,128)S(1)} all-gather(f32[32,4,2]{1,2,0:T(2,128)S(1)} %copy.109), channel_id=3, replica_groups=mesh['kv'=8,'tp'=4] {'kv'}, dimensions={0}, use_global_device_ids=true | all-gather | bytes 9216 | tf_op jit(solution)/shard_map/all_gather | solution.py:14
  274.5 30.9 %all-gather.4 = f32[256,4,2]{1,2,0:T(2,128)S(1)} all-gather(f32[32,4,2]{1,2,0:T(2,128)S(1)} %copy.113), channel_id=6, replica_groups=mesh['kv'=8,'tp'=4] {'kv'}, dimensions={0}, use_global_device_ids=true | all-gather | bytes 9216 | tf_op jit(solution)/shard_map/all_gather | solution.py:14
  305.4 31.0 %all-gather = f32[256,4,2]{1,2,0:T(2,128)S(1)} all-gather(f32[32,4,2]{1,2,0:T(2,128)S(1)} %copy.108), channel_id=2, replica_groups=mesh['kv'=8,'tp'=4] {'kv'}, dimensions={0}, use_global_device_ids=true | all-gather | bytes 9216 | tf_op jit(solution)/shard_map/all_gather | solution.py:14
  337.1 31.1 %all-gather.3 = f32[256,4,2]{1,2,0:T(2,128)S(1)} all-gather(f32[32,4,2]{1,2,0:T(2,128)S(1)} %copy.112), channel_id=5, replica_groups=mesh['kv'=8,'tp'=4] {'kv'}, dimensions={0}, use_global_device_ids=true | all-gather | bytes 9216 | tf_op jit(solution)/shard_map/all_gather | solution.py:14
  369.0 8.8 %fusion.22 = f32[32,4,2,64]{3,2,1,0:T(2,128)} fusion(bf16[32,1024,4,64]{1,3,2,0:T(8,128)(2,1)} %bitcast.68, f32[32,4,2,1024]{3,2,1,0:T(2,128)S(1)} %get-tuple-element.178, f32[32,4,2]{2,1,0:T(4,128)S(1)} %get-tuple-element.177), kind=kOutput, calls=%fused_computation.32 | convolution fusion | flops 34078720 | bytes 17892352 | tf_op jit(solution)/shard_map/bkgp,bpkd->bkgd/dot_general | solution.py:79
  377.8 8.2 %fusion.24 = f32[32,4,2,64]{3,2,1,0:T(2,128)S(1)} fusion(bf16[32,1024,4,64]{1,3,2,0:T(8,128)(2,1)} %bitcast.69, f32[32,4,2,1024]{3,2,1,0:T(2,128)S(1)} %get-tuple-element.176, f32[32,4,2]{2,1,0:T(4,128)S(1)} %get-tuple-element.175), kind=kOutput, calls=%fused_computation.33 | convolution fusion | flops 34078720 | bytes 17892352 | tf_op jit(solution)/shard_map/bkgp,bpkd->bkgd/dot_general | solution.py:79
  386.0 32.9 %all-gather.5 = f32[256,4,2,64]{3,1,2,0:T(4,128)S(1)} all-gather(f32[32,4,2,64]{3,1,2,0:T(4,128)S(1)} %copy.114), channel_id=7, replica_groups=mesh['kv'=8,'tp'=4] {'kv'}, dimensions={0}, use_global_device_ids=true | all-gather | bytes 589824 | tf_op jit(solution)/shard_map/all_gather | solution.py:14
  419.8 32.1 %all-gather.2 = f32[256,4,2,64]{3,1,2,0:T(4,128)S(1)} all-gather(f32[32,4,2,64]{3,1,2,0:T(4,128)S(1)} %copy.111), channel_id=4, replica_groups=mesh['kv'=8,'tp'=4] {'kv'}, dimensions={0}, use_global_device_ids=true | all-gather | bytes 589824 | tf_op jit(solution)/shard_map/all_gather | solution.py:14
  457.6 11.1 %while.20 = (s32[]{:T(128)}, f32[32,4,2]{0,2,1:T(2,128)S(1)}, f32[32,4,2]{0,2,1:T(2,128)S(1)}, f32[32,4,2,64]{3,2,1,0:T(2,128)S(1)}, f32[32,4,2]{0,2,1:T(2,128)S...) while((s32[]{:T(128)}, f32[32,4,2]{0,2,1:T(2,128)S(1)}, ...), condition=%wide.region_13.14_spmd, body=%wide.region_12.13_spmd.sunk | while | flops 101378 | bytes 684189 | solution.py:17
  470.9 31.2 %all-reduce.13.cloned.1.call-done = f32[32,512]{1,0:T(8,128)} async-done(((f32[32,512]{1,0:T(8,128)}), f32[32,512]{1,0:T(8,128)}) %all-reduce.13.cloned.1.call-update) | async-done | bytes 65552 | tf_op jit(solution)/shard_map/psum | solution.py:103
  506.2 3.3 fusion.47
  509.6 21.5 %psum.85 = f32[32,1]{0,1:T(1,128)S(1)} all-reduce(f32[32,1]{0,1:T(1,128)S(1)} %bitcast.78), channel_id=1, replica_groups=mesh['kv'=8,'tp'=4] {'kv'}, use_global_device_ids=true, to_apply=%region_18.19 | all-reduce | flops 32 | bytes 256 | tf_op jit(solution)/shard_map/psum | solution.py:22
  531.1 53.4 %all-reduce.17.cloned.1.call-done = (f32[32,2816]{1,0:T(8,128)}, f32[32,2816]{1,0:T(8,128)}) async-done(((f32[32,2816]{1,0:T(8,128)}, f32[32,2816]{1,0:T(8,128)}), (f32[32,2816]{1,0:T(8,128)}, f32[32,2816]{1,0:T(8,128)})) %all-reduce.17.cloned.1.call-update) | async-done | bytes 720912 | tf_op jit(solution)/shard_map/psum | solution.py:31
  584.5 3.3 fusion.29
  587.8 30.8 %all-reduce.15.cloned.1.call-done = f32[32,512]{1,0:T(8,128)} async-done(((f32[32,512]{1,0:T(8,128)}), f32[32,512]{1,0:T(8,128)}) %all-reduce.15.cloned.1.call-update) | async-done | bytes 65552 | tf_op jit(solution)/shard_map/psum | solution.py:35
  (170 shorter events, 39.4 us)
Async XLA Ops:
  6.5 86.6 %all-reduce.19.cloned.1.call-start = ((), (), s32[]{:S(2)}) async-start(), calls=%async_computation.5 | async-start | bytes 1441792 | tf_op jit(solution)/shard_map/psum | solution.py:31
  15.0 78.1 %copy-start.3 = (bf16[2816,512]{1,0:T(8,128)(2,1)S(1)}, bf16[2816,512]{1,0:T(8,128)(2,1)}, u32[]{:S(2)}) copy-start(bf16[2816,512]{1,0:T(8,128)(2,1)} %param.22) | copy-start | bytes 8650756
  16.4 79.2 %copy-start.16 = (f32[8]{0:T(128)S(1)}, f32[8]{0:T(128)}, u32[]{:S(2)}) copy-start(f32[8]{0:T(128)} %param.27) | copy-start | bytes 100
  16.4 124.3 %all-reduce.9.cloned.1.call-start = ((), (), s32[]{:S(2)}) async-start(), calls=%async_computation | async-start | bytes 131072 | tf_op jit(solution)/shard_map/psum | solution.py:35
  95.5 134.1 %all-reduce.11.cloned.1.call-start = ((), (), s32[]{:S(2)}) async-start(), calls=%async_computation.1 | async-start | bytes 131072 | tf_op jit(solution)/shard_map/psum | solution.py:60
  118.2 43.1 %copy-start.10 = (bf16[512,512]{1,0:T(8,128)(2,1)S(1)}, bf16[512,512]{1,0:T(8,128)(2,1)}, u32[]{:S(2)}) copy-start(bf16[512,512]{1,0:T(8,128)(2,1)} %param.24) | copy-start | bytes 1572868
  118.2 43.1 %copy-start.14 = (f32[512]{0:T(512)S(1)}, f32[512]{0:T(512)}, u32[]{:S(2)}) copy-start(f32[512]{0:T(512)} %param.23) | copy-start | bytes 6148
  163.0 339.1 %all-reduce.13.cloned.1.call-start = ((), (), s32[]{:S(2)}) async-start(), calls=%async_computation.2 | async-start | bytes 131072 | tf_op jit(solution)/shard_map/psum | solution.py:103
  272.9 104.9 %copy-start.4 = (f32[256,4,2]{1,2,0:T(2,128)}, f32[256,4,2]{1,2,0:T(2,128)S(1)}, u32[]{:S(2)}) copy-start(f32[256,4,2]{1,2,0:T(2,128)S(1)} %all-gather.1) | copy-start | bytes 24580
  305.4 72.4 %copy-start.5 = (f32[256,4,2]{1,2,0:T(2,128)}, f32[256,4,2]{1,2,0:T(2,128)S(1)}, u32[]{:S(2)}) copy-start(f32[256,4,2]{1,2,0:T(2,128)S(1)} %all-gather.4) | copy-start | bytes 24580
  336.4 41.4 %copy-start.6 = (f32[256,4,2]{1,2,0:T(2,128)}, f32[256,4,2]{1,2,0:T(2,128)S(1)}, u32[]{:S(2)}) copy-start(f32[256,4,2]{1,2,0:T(2,128)S(1)} %all-gather) | copy-start | bytes 24580
  418.9 33.8 %slice-start = ((f32[256,4,2]{1,2,0:T(2,128)}), f32[32,4,2]{1,2,0:T(2,128)S(1)}, s32[]{:S(2)}) async-start(f32[256,4,2]{1,2,0:T(2,128)} %copy-done.4), calls=%async_computation.6 | async-start | bytes 65536 | tf_op jit(solution)/shard_map/slice | solution.py:15
  418.9 33.9 %slice-start.1 = ((f32[256,4,2]{1,2,0:T(2,128)}), f32[224,4,2]{1,2,0:T(2,128)S(1)}, s32[]{:S(2)}) async-start(f32[256,4,2]{1,2,0:T(2,128)} %copy-done.4), calls=%async_computation.7 | async-start | bytes 458752 | tf_op jit(solution)/shard_map/slice | solution.py:16
  419.5 33.4 %slice-start.2 = ((f32[256,4,2]{1,2,0:T(2,128)}), f32[32,4,2]{1,2,0:T(2,128)S(1)}, s32[]{:S(2)}) async-start(f32[256,4,2]{1,2,0:T(2,128)} %copy-done.5), calls=%async_computation.8 | async-start | bytes 65536 | tf_op jit(solution)/shard_map/slice | solution.py:15
  419.6 33.5 %slice-start.3 = ((f32[256,4,2]{1,2,0:T(2,128)}), f32[224,4,2]{1,2,0:T(2,128)S(1)}, s32[]{:S(2)}) async-start(f32[256,4,2]{1,2,0:T(2,128)} %copy-done.5), calls=%async_computation.9 | async-start | bytes 458752 | tf_op jit(solution)/shard_map/slice | solution.py:16
  419.6 33.6 %slice-start.4 = ((f32[256,4,2]{1,2,0:T(2,128)}), f32[32,4,2]{1,2,0:T(2,128)S(1)}, s32[]{:S(2)}) async-start(f32[256,4,2]{1,2,0:T(2,128)} %copy-done.6), calls=%async_computation.10 | async-start | bytes 65536 | tf_op jit(solution)/shard_map/slice | solution.py:15
  419.6 34.8 %slice-start.5 = ((f32[256,4,2]{1,2,0:T(2,128)}), f32[32,4,2]{1,2,0:T(2,128)S(1)}, s32[]{:S(2)}) async-start(f32[256,4,2]{1,2,0:T(2,128)} %copy-done.7), calls=%async_computation.11 | async-start | bytes 65536 | tf_op jit(solution)/shard_map/slice | solution.py:15
  457.5 12.1 %copy-start.15 = (f32[64]{0:T(128)S(1)}, f32[64]{0:T(128)}, u32[]{:S(2)}) copy-start(f32[64]{0:T(128)} %param.28) | copy-start | bytes 772
  457.5 12.5 %copy-start.9 = (bf16[512,512]{1,0:T(8,128)(2,1)S(1)}, bf16[512,512]{1,0:T(8,128)(2,1)}, u32[]{:S(2)}) copy-start(bf16[512,512]{1,0:T(8,128)(2,1)} %param.29) | copy-start | bytes 1572868
  457.5 44.6 %copy-start.8 = (f32[32,512]{1,0:T(8,128)S(1)}, f32[32,512]{1,0:T(8,128)}, u32[]{:S(2)}) copy-start(f32[32,512]{1,0:T(8,128)} %all-reduce.9.cloned.1.call-done) | copy-start | bytes 196612
  457.6 45.5 %copy-start.13 = (f32[512]{0:T(512)S(1)}, f32[512]{0:T(512)}, u32[]{:S(2)}) copy-start(f32[512]{0:T(512)} %param.30) | copy-start | bytes 6148
  470.9 113.6 %all-reduce.17.cloned.1.call-start = ((), (), s32[]{:S(2)}) async-start(), calls=%async_computation.4 | async-start | bytes 1441792 | tf_op jit(solution)/shard_map/psum | solution.py:31
  506.2 113.8 %copy-start.1 = (bf16[512,2816]{1,0:T(8,128)(2,1)S(1)}, bf16[512,2816]{1,0:T(8,128)(2,1)}, u32[]{:S(2)}) copy-start(bf16[512,2816]{1,0:T(8,128)(2,1)} %param.21) | copy-start | bytes 8650756
  509.6 109.1 %all-reduce.15.cloned.1.call-start = ((), (), s32[]{:S(2)}) async-start(), calls=%async_computation.3 | async-start | bytes 131072 | tf_op jit(solution)/shard_map/psum | solution.py:35
  (5 other events, 41.2 us)
Sparse Core Ops, SparseCore 0:
  16.5 76.5 all-reduce.18
  95.6 30.6 all-reduce.8
  163.1 66.4 all-reduce.10
  471.0 31.0 all-reduce.12
  509.7 74.7 all-reduce.16
  588.0 30.6 all-reduce.14
where the time goes:
time: 629 us; the launch traced here: 627 us
  blocking collectives  259 us (41%)
  waiting for transfers between devices  236 us (38%)
  local copies, waits for them, and re-layouts  58.6 us (9%)
  matrix products  44.7 us (7%)
  other arithmetic  14.3 us (2%)
  between operations  13.7 us (2%)
    all_gather x6, blocking collectives, merged(): pieces = jax.tree.map(lambda part: lax.all_gather(part, axis), value)  189 us
    psum x2, waiting for transfers between devices, channel_mixer(): gate_sum, up_sum = lax.psum((part_gate, part_up), 'kv')  107 us
    psum x1, waiting for transfers between devices, attention_mix(): queries = lax.psum(part_query, 'kv')  66.6 us
    psum x3, blocking collectives, norm_total(): return lax.psum(squares, 'kv')  63.8 us
    unnamed x36, local copies, waits for them, and re-layouts  45.2 us
    psum x1, waiting for transfers between devices, attention_mix(): return lax.psum(partial_value, 'tp')  31.2 us
    psum x2, waiting for transfers between devices, channel_mixer(): return lax.psum(partial_value, 'tp')  30.8 us
    dot_general x2, matrix products, partial_map(): jnp.einsum('bkgp,bpkd->bkgd', exp_terms.astype(jnp.bfloat16), stored, pre...  16.9 us
  transfers between devices with their start and end apart: 6, of which 5 were waited for; matrix products, arithmetic and copies ran while one was open for 7% of the time, Pallas kernels for 0%

commit v1 on v0

--- a/solution.py
+++ b/solution.py
@@ -8,6 +8,14 @@
 HEAD = 64
 EPS = 1e-06
 HEAD_SCALE = 0.8
+
+
+def doubling_sum(value, axis):
+    size, summed = (lax.axis_size(axis), value)
+    for far in [1 << k for k in range(size.bit_length() - 1)]:
+        pairs = [(i, i ^ far) for i in range(size)]
+        summed = summed + lax.ppermute(summed, axis, pairs)
+    return summed
 
 
 def merged(value, axis, join):
@@ -57,7 +65,7 @@
     scaled = (residual * mix_gain).astype(jnp.bfloat16)
     part_query = jnp.dot(scaled, w_query, preferred_element_type=jnp.float32)
     row_total = norm_total(squares)
-    queries = lax.psum(part_query, "kv")
+    queries = doubling_sum(part_query, "kv")
     queries = (queries * lax.rsqrt(row_total / D + EPS)).astype(jnp.bfloat16)
     batch_rows = queries.shape[0]
     kv_local = key_cache.shape[2] // HEAD

time: 629 us -> 596 us (0.948)
  waiting for transfers between devices: 236 us -> 202 us
    psum x1 -> x0, waiting for transfers between devices: 66.6 us -> none  [attention_mix(): queries = lax.psum(part_query, 'kv')]
    psum x2, waiting for transfers between devices: 30.8 us -> 61.6 us  [channel_mixer(): return lax.psum(partial_value, 'tp')]
    unnamed x36 -> x38, local copies, waits for them, and re-layouts: 45.2 us -> 45.1 us
  transfers between devices with their start and end apart: 6 -> 8, of which waited for: 5 -> 6; matrix products, arithmetic and copies ran while one was open for 7% -> 8% of each run, Pallas kernels for 0% -> 0%
where the time goes in v1:
time: 596 us; the launch traced here: 594 us
  blocking collectives  260 us (44%)
  waiting for transfers between devices  202 us (34%)
  local copies, waits for them, and re-layouts  58.5 us (10%)
  matrix products  44.2 us (7%)
  between operations  13.4 us (2%)
  other arithmetic  12.6 us (2%)
    all_gather x6, blocking collectives, merged(): pieces = jax.tree.map(lambda part: lax.all_gather(part, axis), value)  190 us
    psum x2, waiting for transfers between devices, channel_mixer(): gate_sum, up_sum = lax.psum((part_gate, part_up), 'kv')  107 us
    psum x3, blocking collectives, norm_total(): return lax.psum(squares, 'kv')  63.8 us
    psum x2, waiting for transfers between devices, channel_mixer(): return lax.psum(partial_value, 'tp')  61.6 us
    unnamed x38, local copies, waits for them, and re-layouts  45.1 us
    psum x1, waiting for transfers between devices, attention_mix(): return lax.psum(partial_value, 'tp')  27.9 us
    dot_general x2, matrix products, partial_map(): jnp.einsum('bkgp,bpkd->bkgd', exp_terms.astype(jnp.bfloat16), stored, pre...  16.9 us
  transfers between devices with their start and end apart: 8, of which 6 were waited for; matrix products, arithmetic and copies ran while one was open for 8% of the time, Pallas kernels for 0%

profile of v1, /device:TPU:0, one launch (start us, length us, event | category | flops | bytes accessed | tf_op | source)
XLA Modules:
  0.0 594.1 jit_solution(11337261283790991541)
XLA Ops:
  6.5 6.5 %all_gather.39 = bf16[32,512]{1,0:T(8,128)(2,1)S(1)} all-gather(bf16[32,128]{1,0:T(8,128)(2,1)} %param.18), channel_id=1, replica_groups=mesh['kv'=8,'tp'=4] {'tp'}, dimensions={1}, use_global_device_ids=true | all-gather | bytes 40960 | tf_op jit(solution)/shard_map/all_gather | solution.py:132
  16.6 22.7 %psum.71 = f32[32,1]{0,1:T(1,128)S(1)} all-reduce(f32[32,1]{0,1:T(1,128)S(1)} %bitcast.79), channel_id=1, replica_groups=mesh['kv'=8,'tp'=4] {'kv'}, use_global_device_ids=true, to_apply=%region_2.0 | all-reduce | flops 32 | bytes 256 | tf_op jit(solution)/shard_map/psum | solution.py:30
  39.3 53.8 %all-reduce.16.cloned.1.call-done = (f32[32,2816]{1,0:T(8,128)}, f32[32,2816]{1,0:T(8,128)}) async-done(((f32[32,2816]{1,0:T(8,128)}, f32[32,2816]{1,0:T(8,128)}), (f32[32,2816]{1,0:T(8,128)}, f32[32,2816]{1,0:T(8,128)})) %all-reduce.16.cloned.1.call-update) | async-done | bytes 720912 | tf_op jit(solution)/shard_map/psum | solution.py:39
  95.6 30.8 %all-reduce.8.cloned.1.call-done = f32[32,512]{1,0:T(8,128)} async-done(((f32[32,512]{1,0:T(8,128)}), f32[32,512]{1,0:T(8,128)}) %all-reduce.8.cloned.1.call-update) | async-done | bytes 65552 | tf_op jit(solution)/shard_map/psum | solution.py:43
  129.0 22.5 %copy.107 = bf16[32,1024,256]{1,2,0:T(8,128)(2,1)} copy(bf16[32,1024,256]{2,1,0:T(8,128)(2,1)} %param.25) | data formatting | bytes 33554432 | tf_op args[7]
  151.5 22.5 %copy.110 = bf16[32,1024,256]{1,2,0:T(8,128)(2,1)} copy(bf16[32,1024,256]{2,1,0:T(8,128)(2,1)} %param.26) | data formatting | bytes 33554432 | tf_op args[8]
  175.7 19.6 %psum.74 = f32[32,1]{0,1:T(1,128)S(1)} all-reduce(f32[32,1]{0,1:T(1,128)S(1)} %bitcast.80), channel_id=1, replica_groups=mesh['kv'=8,'tp'=4] {'kv'}, use_global_device_ids=true, to_apply=%region_6.7 | all-reduce | flops 32 | bytes 256 | tf_op jit(solution)/shard_map/psum | solution.py:30
  195.4 5.1 collective-permute-done.2
  200.7 4.9 fusion.55
  205.6 4.9 fusion.54
  212.1 30.8 %all-gather.1 = f32[256,4,2]{1,2,0:T(2,128)S(1)} all-gather(f32[32,4,2]{1,2,0:T(2,128)S(1)} %copy.109), channel_id=3, replica_groups=mesh['kv'=8,'tp'=4] {'kv'}, dimensions={0}, use_global_device_ids=true | all-gather | bytes 9216 | tf_op jit(solution)/shard_map/all_gather | solution.py:22
  244.5 30.9 %all-gather.4 = f32[256,4,2]{1,2,0:T(2,128)S(1)} all-gather(f32[32,4,2]{1,2,0:T(2,128)S(1)} %copy.113), channel_id=6, replica_groups=mesh['kv'=8,'tp'=4] {'kv'}, dimensions={0}, use_global_device_ids=true | all-gather | bytes 9216 | tf_op jit(solution)/shard_map/all_gather | solution.py:22
  275.3 30.7 %all-gather = f32[256,4,2]{1,2,0:T(2,128)S(1)} all-gather(f32[32,4,2]{1,2,0:T(2,128)S(1)} %copy.108), channel_id=2, replica_groups=mesh['kv'=8,'tp'=4] {'kv'}, dimensions={0}, use_global_device_ids=true | all-gather | bytes 9216 | tf_op jit(solution)/shard_map/all_gather | solution.py:22
  306.8 31.3 %all-gather.3 = f32[256,4,2]{1,2,0:T(2,128)S(1)} all-gather(f32[32,4,2]{1,2,0:T(2,128)S(1)} %copy.112), channel_id=5, replica_groups=mesh['kv'=8,'tp'=4] {'kv'}, dimensions={0}, use_global_device_ids=true | all-gather | bytes 9216 | tf_op jit(solution)/shard_map/all_gather | solution.py:22
  338.8 8.8 %fusion.22 = f32[32,4,2,64]{3,2,1,0:T(2,128)} fusion(bf16[32,1024,4,64]{1,3,2,0:T(8,128)(2,1)} %bitcast.68, f32[32,4,2,1024]{3,2,1,0:T(2,128)S(1)} %get-tuple-element.178, f32[32,4,2]{2,1,0:T(4,128)S(1)} %get-tuple-element.177), kind=kOutput, calls=%fused_computation.32 | convolution fusion | flops 34078720 | bytes 17892352 | tf_op jit(solution)/shard_map/bkgp,bpkd->bkgd/dot_general | solution.py:87
  347.6 8.2 %fusion.24 = f32[32,4,2,64]{3,2,1,0:T(2,128)S(1)} fusion(bf16[32,1024,4,64]{1,3,2,0:T(8,128)(2,1)} %bitcast.69, f32[32,4,2,1024]{3,2,1,0:T(2,128)S(1)} %get-tuple-element.176, f32[32,4,2]{2,1,0:T(4,128)S(1)} %get-tuple-element.175), kind=kOutput, calls=%fused_computation.33 | convolution fusion | flops 34078720 | bytes 17892352 | tf_op jit(solution)/shard_map/bkgp,bpkd->bkgd/dot_general | solution.py:87
  355.8 33.5 %all-gather.5 = f32[256,4,2,64]{3,1,2,0:T(4,128)S(1)} all-gather(f32[32,4,2,64]{3,1,2,0:T(4,128)S(1)} %copy.114), channel_id=7, replica_groups=mesh['kv'=8,'tp'=4] {'kv'}, dimensions={0}, use_global_device_ids=true | all-gather | bytes 589824 | tf_op jit(solution)/shard_map/all_gather | solution.py:22
  390.2 32.6 %all-gather.2 = f32[256,4,2,64]{3,1,2,0:T(4,128)S(1)} all-gather(f32[32,4,2,64]{3,1,2,0:T(4,128)S(1)} %copy.111), channel_id=4, replica_groups=mesh['kv'=8,'tp'=4] {'kv'}, dimensions={0}, use_global_device_ids=true | all-gather | bytes 589824 | tf_op jit(solution)/shard_map/all_gather | solution.py:22
  428.5 11.1 %while.20 = (s32[]{:T(128)}, f32[32,4,2]{0,2,1:T(2,128)S(1)}, f32[32,4,2]{0,2,1:T(2,128)S(1)}, f32[32,4,2,64]{3,2,1,0:T(2,128)S(1)}, f32[32,4,2]{0,2,1:T(2,128)S...) while((s32[]{:T(128)}, f32[32,4,2]{0,2,1:T(2,128)S(1)}, ...), condition=%wide.region_12.13_spmd, body=%wide.region_11.12_spmd.sunk | while | flops 101378 | bytes 684189 | solution.py:25
  441.8 27.9 %all-reduce.10.cloned.1.call-done = f32[32,512]{1,0:T(8,128)} async-done(((f32[32,512]{1,0:T(8,128)}), f32[32,512]{1,0:T(8,128)}) %all-reduce.10.cloned.1.call-update) | async-done | bytes 65552 | tf_op jit(solution)/shard_map/psum | solution.py:111
  477.3 21.6 %psum.77 = f32[32,1]{0,1:T(1,128)S(1)} all-reduce(f32[32,1]{0,1:T(1,128)S(1)} %bitcast.78), channel_id=1, replica_groups=mesh['kv'=8,'tp'=4] {'kv'}, use_global_device_ids=true, to_apply=%region_17.18 | all-reduce | flops 32 | bytes 256 | tf_op jit(solution)/shard_map/psum | solution.py:30
  498.9 53.2 %all-reduce.14.cloned.1.call-done = (f32[32,2816]{1,0:T(8,128)}, f32[32,2816]{1,0:T(8,128)}) async-done(((f32[32,2816]{1,0:T(8,128)}, f32[32,2816]{1,0:T(8,128)}), (f32[32,2816]{1,0:T(8,128)}, f32[32,2816]{1,0:T(8,128)})) %all-reduce.14.cloned.1.call-update) | async-done | bytes 720912 | tf_op jit(solution)/shard_map/psum | solution.py:39
  552.1 3.3 fusion.29
  555.5 30.8 %all-reduce.12.cloned.1.call-done = f32[32,512]{1,0:T(8,128)} async-done(((f32[32,512]{1,0:T(8,128)}), f32[32,512]{1,0:T(8,128)}) %all-reduce.12.cloned.1.call-update) | async-done | bytes 65552 | tf_op jit(solution)/shard_map/psum | solution.py:43
  (177 shorter events, 43.5 us)
Async XLA Ops:
  6.5 86.6 %all-reduce.16.cloned.1.call-start = ((), (), s32[]{:S(2)}) async-start(), calls=%async_computation.4 | async-start | bytes 1441792 | tf_op jit(solution)/shard_map/psum | solution.py:39
  15.1 78.1 %copy-start.3 = (bf16[2816,512]{1,0:T(8,128)(2,1)S(1)}, bf16[2816,512]{1,0:T(8,128)(2,1)}, u32[]{:S(2)}) copy-start(bf16[2816,512]{1,0:T(8,128)(2,1)} %param.22) | copy-start | bytes 8650756
  16.4 109.9 %copy-start.11 = (bf16[512,512]{1,0:T(8,128)(2,1)S(1)}, bf16[512,512]{1,0:T(8,128)(2,1)}, u32[]{:S(2)}) copy-start(bf16[512,512]{1,0:T(8,128)(2,1)} %param.24) | copy-start | bytes 1572868
  16.4 109.9 %copy-start.15 = (f32[512]{0:T(512)S(1)}, f32[512]{0:T(512)}, u32[]{:S(2)}) copy-start(f32[512]{0:T(512)} %param.23) | copy-start | bytes 6148
  16.4 112.4 %copy-start.17 = (f32[8]{0:T(128)S(1)}, f32[8]{0:T(128)}, u32[]{:S(2)}) copy-start(f32[8]{0:T(128)} %param.27) | copy-start | bytes 100
  16.5 109.9 %all-reduce.8.cloned.1.call-start = ((), (), s32[]{:S(2)}) async-start(), calls=%async_computation | async-start | bytes 131072 | tf_op jit(solution)/shard_map/psum | solution.py:43
  95.5 374.2 %all-reduce.10.cloned.1.call-start = ((), (), s32[]{:S(2)}) async-start(), calls=%async_computation.1 | async-start | bytes 131072 | tf_op jit(solution)/shard_map/psum | solution.py:111
  127.4 46.6 %collective-permute-start = (f32[32,512]{1,0:T(8,128)S(1)}, f32[32,512]{1,0:T(8,128)S(1)}, u32[]{:S(2)}, u32[]{:S(2)}) collective-permute-start(f32[32,512]{1,0:T(8,128)S(1)} %fusion.38), channel_id=1, source_target_pairs={{0,4},{4,0},{8,12},{12,8},{16,20},{20,16},{24,28},{28,24},{1,5},{5... | collective-permute-start | bytes 196616 | tf_op jit(solution)/shard_map/ppermute | solution.py:17
  174.0 21.3 %collective-permute-start.1 = (f32[32,512]{1,0:T(8,128)S(1)}, f32[32,512]{1,0:T(8,128)S(1)}, u32[]{:S(2)}, u32[]{:S(2)}) collective-permute-start(f32[32,512]{1,0:T(8,128)S(1)} %add.86), channel_id=1, source_target_pairs={{0,8},{4,12},{8,0},{12,4},{16,24},{20,28},{24,16},{28,20},{1,9},{5... | collective-permute-start | bytes 196616 | tf_op jit(solution)/shard_map/ppermute | solution.py:17
  195.3 5.2 collective-permute-start.2
  242.9 104.7 %copy-start.4 = (f32[256,4,2]{1,2,0:T(2,128)}, f32[256,4,2]{1,2,0:T(2,128)S(1)}, u32[]{:S(2)}) copy-start(f32[256,4,2]{1,2,0:T(2,128)S(1)} %all-gather.1) | copy-start | bytes 24580
  275.3 72.3 %copy-start.5 = (f32[256,4,2]{1,2,0:T(2,128)}, f32[256,4,2]{1,2,0:T(2,128)S(1)}, u32[]{:S(2)}) copy-start(f32[256,4,2]{1,2,0:T(2,128)S(1)} %all-gather.4) | copy-start | bytes 24580
  306.1 41.5 %copy-start.6 = (f32[256,4,2]{1,2,0:T(2,128)}, f32[256,4,2]{1,2,0:T(2,128)S(1)}, u32[]{:S(2)}) copy-start(f32[256,4,2]{1,2,0:T(2,128)S(1)} %all-gather) | copy-start | bytes 24580
  389.3 34.3 %slice-start = ((f32[256,4,2]{1,2,0:T(2,128)}), f32[32,4,2]{1,2,0:T(2,128)S(1)}, s32[]{:S(2)}) async-start(f32[256,4,2]{1,2,0:T(2,128)} %copy-done.4), calls=%async_computation.5 | async-start | bytes 65536 | tf_op jit(solution)/shard_map/slice | solution.py:23
  389.3 34.4 %slice-start.1 = ((f32[256,4,2]{1,2,0:T(2,128)}), f32[224,4,2]{1,2,0:T(2,128)S(1)}, s32[]{:S(2)}) async-start(f32[256,4,2]{1,2,0:T(2,128)} %copy-done.4), calls=%async_computation.6 | async-start | bytes 458752 | tf_op jit(solution)/shard_map/slice | solution.py:24
  390.0 33.9 %slice-start.2 = ((f32[256,4,2]{1,2,0:T(2,128)}), f32[32,4,2]{1,2,0:T(2,128)S(1)}, s32[]{:S(2)}) async-start(f32[256,4,2]{1,2,0:T(2,128)} %copy-done.5), calls=%async_computation.7 | async-start | bytes 65536 | tf_op jit(solution)/shard_map/slice | solution.py:23
  390.0 34.0 %slice-start.3 = ((f32[256,4,2]{1,2,0:T(2,128)}), f32[224,4,2]{1,2,0:T(2,128)S(1)}, s32[]{:S(2)}) async-start(f32[256,4,2]{1,2,0:T(2,128)} %copy-done.5), calls=%async_computation.8 | async-start | bytes 458752 | tf_op jit(solution)/shard_map/slice | solution.py:24
  390.0 34.1 %slice-start.4 = ((f32[256,4,2]{1,2,0:T(2,128)}), f32[32,4,2]{1,2,0:T(2,128)S(1)}, s32[]{:S(2)}) async-start(f32[256,4,2]{1,2,0:T(2,128)} %copy-done.6), calls=%async_computation.9 | async-start | bytes 65536 | tf_op jit(solution)/shard_map/slice | solution.py:23
  390.0 35.3 %slice-start.5 = ((f32[256,4,2]{1,2,0:T(2,128)}), f32[32,4,2]{1,2,0:T(2,128)S(1)}, s32[]{:S(2)}) async-start(f32[256,4,2]{1,2,0:T(2,128)} %copy-done.7), calls=%async_computation.10 | async-start | bytes 65536 | tf_op jit(solution)/shard_map/slice | solution.py:23
  428.5 41.3 %copy-start.9 = (f32[32,512]{1,0:T(8,128)S(1)}, f32[32,512]{1,0:T(8,128)}, u32[]{:S(2)}) copy-start(f32[32,512]{1,0:T(8,128)} %all-reduce.8.cloned.1.call-done) | copy-start | bytes 196612
  428.5 42.3 %copy-start.14 = (f32[512]{0:T(512)S(1)}, f32[512]{0:T(512)}, u32[]{:S(2)}) copy-start(f32[512]{0:T(512)} %param.30) | copy-start | bytes 6148
  441.8 110.3 %all-reduce.14.cloned.1.call-start = ((), (), s32[]{:S(2)}) async-start(), calls=%async_computation.3 | async-start | bytes 1441792 | tf_op jit(solution)/shard_map/psum | solution.py:39
  473.9 113.7 %copy-start.1 = (bf16[512,2816]{1,0:T(8,128)(2,1)S(1)}, bf16[512,2816]{1,0:T(8,128)(2,1)}, u32[]{:S(2)}) copy-start(bf16[512,2816]{1,0:T(8,128)(2,1)} %param.21) | copy-start | bytes 8650756
  477.3 109.0 %all-reduce.12.cloned.1.call-start = ((), (), s32[]{:S(2)}) async-start(), calls=%async_computation.2 | async-start | bytes 131072 | tf_op jit(solution)/shard_map/psum | solution.py:43
  (8 other events, 89.9 us)
Sparse Core Ops, SparseCore 0:
  16.6 76.5 all-reduce.15
  95.7 30.6 all-reduce.7
  441.9 27.8 all-reduce.9
  477.4 74.6 all-reduce.13
  555.6 30.6 all-reduce.11
